TPU v7x, 32 devices: a whole 2x2x4 slice. The times are simulated.
32 devices in a mesh: fs: 4 (over z), rep: 4 (over y, x), tp: 2 (over core).
Axes of the slice: x: 2, y: 2, z: 4, core: 2. Of those that a mesh axis runs over, the one named last changes fastest.
Arguments:
- first_mix: bfloat16 [12288, 2048], P(('fs', 'rep'), 'tp'), may hold values from -6 to 6
- second_mix: bfloat16 [12288, 2048], P(('fs', 'rep'), 'tp'), may hold values from -6 to 6
- lambda_head: float32 [8], P('tp'), may hold values from 0.3 to 0.8
- head_gain: float32 [256], replicated, may hold values from 0.1 to 1.9
- out_cotangent: bfloat16 [12288, 2048], P(('fs', 'rep')), may hold values from -0.053955078 to 0.053955078
- basis: bfloat16 [2048, 256], P('tp'), may hold values from -0.125 to 0.125
- weight: float32 [2048, 2048], P('tp', 'fs'), may hold values from -3 to 3
- first_moment: float32 [2048, 256], P('fs', 'tp'), may hold values from -4.5 to 4.5
- second_moment: float32 [2048, 256], P('fs', 'tp'), may hold values from 0.05 to 0.5
Outputs:
- weight_new: float32 [2048, 2048], P('tp', 'fs')
- weight_copy: bfloat16 [2048, 2048], P('tp')
- step_out: float32 [2048, 2048], P('tp', 'fs')
- first_new: float32 [2048, 256], P('fs', 'tp')
- second_new: float32 [2048, 256], P('fs', 'tp')
All inputs are finite; a program needn't handle non-finite values.
Results may differ from a plain program's by a relative error of at most 0.0075.
Values may be sent and summed in bfloat16 or wider, within the bound.
A program may use at most 64 MiB of HBM per device.

v0:
```python
import jax
import jax.numpy as jnp
from jax import lax
from jax.sharding import PartitionSpec as P

out_scale = 0.8
beta_first = 0.9
beta_second = 0.95


def head_output(first_piece, second_piece, lambdas, head_gain):
    token_count = first_piece.shape[0]
    head_width = head_gain.shape[0]
    head_count = lambdas.shape[0] // head_width
    mixture = first_piece.astype(jnp.float32) - lambdas[None, :] * second_piece.astype(jnp.float32)
    grouped = mixture.reshape(token_count, head_count, head_width)
    inverse = lax.rsqrt(jnp.mean(grouped * grouped, axis=-1, keepdims=True) + 1e-06)
    normed = grouped * inverse * head_gain[None, None, :] * out_scale
    return normed.reshape(token_count, head_count * head_width).astype(jnp.bfloat16)


def split_product(narrow, wide, numbers):
    upper = wide.astype(jnp.bfloat16)
    lower = (wide - upper.astype(jnp.float32)).astype(jnp.bfloat16)
    return lax.dot_general(
        narrow, upper, numbers, preferred_element_type=jnp.float32
    ) + lax.dot_general(narrow, lower, numbers, preferred_element_type=jnp.float32)


def body(
    first_mix,
    second_mix,
    lambda_head,
    head_gain,
    out_cotangent,
    basis,
    weight,
    first_moment,
    second_moment,
):
    lambdas = jnp.repeat(lambda_head, head_gain.shape[0])
    head_out = head_output(first_mix, second_mix, lambdas, head_gain)
    reduced = jnp.dot(head_out, basis, preferred_element_type=jnp.float32)
    proj_rows = lax.psum_scatter(
        split_product(out_cotangent, reduced, (((0,), (0,)), ((), ()))),
        "fs",
        scatter_dimension=0,
        tiled=True,
    )
    proj_rows = lax.psum_scatter(proj_rows, "tp", scatter_dimension=1, tiled=True)
    projected = lax.psum(proj_rows, "rep")
    first_new = beta_first * first_moment + (1.0 - beta_first) * projected
    second_new = beta_second * second_moment + (1.0 - beta_second) * projected * projected
    direction = first_new / (jnp.sqrt(second_new) + 1e-08)
    energy = lax.psum(jnp.sum(direction * direction), ("fs", "tp"))
    entries = direction.shape[0] * direction.shape[1] * lax.axis_size("fs") * lax.axis_size("tp")
    spread = jnp.sqrt(energy / entries)
    full_direction = lax.all_gather(direction, "tp", axis=1, tiled=True)
    step_out = split_product(basis, full_direction, (((1,), (1,)), ((), ()))) * (
        -1.0 / (spread + 1e-06)
    )
    weight_new = weight + step_out
    weight_copy = lax.all_gather(weight_new.astype(jnp.bfloat16), "fs", axis=1, tiled=True)
    return (weight_new, weight_copy, step_out, first_new, second_new)


def solution(mesh):
    return jax.shard_map(
        body,
        mesh=mesh,
        in_specs=(
            P(("fs", "rep"), "tp"),
            P(("fs", "rep"), "tp"),
            P("tp"),
            P(),
            P(("fs", "rep"), None),
            P("tp", None),
            P("tp", "fs"),
            P("fs", "tp"),
            P("fs", "tp"),
        ),
        out_specs=(P("tp", "fs"), P("tp", None), P("tp", "fs"), P("fs", "tp"), P("fs", "tp")),
        check_vma=False,
    )
```

profile of v0, /device:TPU:0, one launch (start us, length us, event | category | flops | bytes accessed | tf_op | source)
XLA Modules:
  0.0 254.0 jit_solution(11689265764747644795)
XLA Ops:
  7.2 0.9 broadcast_bitcast_fusion.1
  8.1 0.7 broadcast_bitcast_fusion
  8.8 4.2 %fusion = f32[768,1024]{1,0:T(8,128)} fusion(bf16[768,1024]{1,0:T(8,128)(2,1)} %param.10, bf16[768,1024]{1,0:T(8,128)(2,1)} %param.9, f32[1024]{0:T(1024)S(1)} %bitcast.19), kind=kLoop, calls=%fused_computation.2 | loop fusion | flops 3932160 | bytes 6295552 | tf_op jit(solution)/shard_map/mul | solution.py:17
  13.0 5.2 %mul.92 = f32[768,4,256]{2,1,0:T(4,128)} reshape(f32[768,1024]{1,0:T(8,128)} %fusion) | data formatting | bytes 6291456 | tf_op jit(solution)/shard_map/mul | solution.py:17
  18.2 2.8 %reduce_sum.18 = f32[768,4]{1,0:T(8,128)S(1)} reduce(f32[768,4,256]{2,1,0:T(4,128)} %mul.92, f32[]{:T(128)} %constant.2.clone.1), dimensions={2}, to_apply=%region_0.0 | reduce | flops 783360 | bytes 3158020 | tf_op jit(solution)/shard_map/reduce_sum | solution.py:17
  21.0 0.1 add_rsqrt_fusion
  21.1 1.0 mul.93
  22.1 0.8 copy.42
  22.8 0.6 copy-done.1
  23.5 0.5 copy-done.2
  23.9 0.1 copy-done.3
  24.0 0.9 fusion.2
  25.0 1.0 fusion.5
  26.0 2.4 fusion.1
  28.5 46.5 %reduce-scatter.3.cloned.1.call-done = f32[512,256]{0,1:T(8,128)} async-done(((f32[2048,256]{0,1:T(8,128)}), f32[512,256]{0,1:T(8,128)}) %reduce-scatter.3.cloned.1.call-update) | async-done | bytes 524304 | tf_op jit(solution)/shard_map/reduce_scatter | solution.py:44
  75.0 9.3 %reduce-scatter.5.cloned.1.call-done = f32[512,128]{0,1:T(8,128)} async-done(((f32[512,256]{0,1:T(8,128)}), f32[512,128]{0,1:T(8,128)}) %reduce-scatter.5.cloned.1.call-update) | async-done | bytes 262160 | tf_op jit(solution)/shard_map/reduce_scatter | solution.py:50
  84.4 0.8 copy.31
  85.2 1.8 copy.34
  87.0 2.9 %copy.35 = f32[1024,512]{0,1:T(8,128)} copy(f32[1024,512]{1,0:T(8,128)} %param.15) | data formatting | bytes 4194304 | tf_op args[6]
  89.9 41.6 %all-reduce.2.cloned.1.call-done = f32[512,128]{0,1:T(8,128)} async-done(((f32[512,128]{0,1:T(8,128)}), f32[512,128]{0,1:T(8,128)}) %all-reduce.2.cloned.1.call-update) | async-done | bytes 262160 | tf_op jit(solution)/shard_map/psum | solution.py:51
  131.5 2.6 %multiply_reduce_fusion = (f32[]{:T(128)}, f32[512,128]{0,1:T(8,128)S(1)}, f32[512,128]{0,1:T(8,128)}, f32[512,128]{0,1:T(8,128)}) fusion(f32[512,128]{0,1:T(8,128)} %all-reduce.2.cloned.1.call-done, f32[512,128]{0,1:T(8,128)} %copy.34, f32[512,128]{0,1:T(8,128)} %copy.31), kind=kLoop, calls=%fused_computation.12 | loop fusion | flops 720895 | bytes 1572868 | tf_op jit(solution)/shard_map/reduce_sum | solution.py:55
  134.1 16.5 %psum.15 = f32[]{:T(128)} all-reduce(f32[]{:T(128)} %get-tuple-element.22), channel_id=1, replica_groups=mesh['fs'=4,'rep'=4,'tp'=2] {'fs','tp'}, use_global_device_ids=true, to_apply=%region_5.0 | all-reduce | flops 1 | bytes 8 | tf_op jit(solution)/shard_map/psum | solution.py:55
  151.3 2.2 all_gather.6
  153.5 0.8 copy-done.4
  154.3 2.8 %fusion.8 = f32[512,1024]{1,0:T(8,128)} fusion(bf16[1024,256]{1,0:T(8,128)(2,1)} %param.14, f32[512,256]{0,1:T(8,128)S(1)} %all_gather.6), kind=kOutput, calls=%fused_computation.19 | convolution fusion | flops 268566528 | bytes 3145728 | tf_op jit(solution)/shard_map/dot_general | solution.py:25
  157.2 5.7 %fusion.11 = (bf16[1024,512]{0,1:T(8,128)(2,1)}, f32[1024,512]{0,1:T(8,128)}, f32[1024,512]{0,1:T(8,128)}) fusion(f32[1024,512]{0,1:T(8,128)} %copy.35, f32[]{:T(128)S(6)} %div.19, f32[512,1024]{1,0:T(8,128)} %fusion.8, bf16[1024,256]{1,0:T(8,128)(2,1)} %param.14, f32[512,256]{0,1:T(8,128)} %copy-done.4), kind=kOutput, calls=%fused_computation.24 | convolution fusion | flops 271056896 | bytes 10485764 | tf_op jit(solution)/shard_map/dot_general | solution.py:27
  162.9 1.8 copy.40
  164.7 0.8 copy.39
  165.5 3.0 %copy.36 = f32[1024,512]{1,0:T(8,128)} copy(f32[1024,512]{0,1:T(8,128)} %get-tuple-element.21) | data formatting | bytes 4194304
  168.5 3.0 %copy.38 = f32[1024,512]{1,0:T(8,128)} copy(f32[1024,512]{0,1:T(8,128)} %get-tuple-element.26) | data formatting | bytes 4194304
  171.5 69.5 %all-gather.2.cloned.1.call-done = bf16[1024,2048]{0,1:T(8,128)(2,1)} async-done(((bf16[1024,512]{0,1:T(8,128)(2,1)}), bf16[1024,2048]{0,1:T(8,128)(2,1)}) %all-gather.2.cloned.1.call-update) | async-done | bytes 4194320 | tf_op jit(solution)/shard_map/all_gather | solution.py:63
  241.0 6.4 %copy.37 = bf16[1024,2048]{1,0:T(8,128)(2,1)} copy(bf16[1024,2048]{0,1:T(8,128)(2,1)} %all-gather.2.cloned.1.call-done) | data formatting | bytes 8388608
  (20 shorter events, 0.3 us)
Async XLA Ops:
  7.2 17.8 %copy-start = (bf16[768,2048]{1,0:T(8,128)(2,1)S(1)}, bf16[768,2048]{1,0:T(8,128)(2,1)}, u32[]{:S(2)}) copy-start(bf16[768,2048]{1,0:T(8,128)(2,1)} %param.13) | copy-start | bytes 9437188
  7.2 67.7 %reduce-scatter.3.cloned.1.call-start = ((), (), s32[]{:S(2)}) async-start(), calls=%async_computation.2 | async-start | bytes 2621440 | tf_op jit(solution)/shard_map/reduce_scatter | solution.py:44
  22.0 1.4 copy-start.1
  22.1 1.9 copy-start.2
  22.1 2.0 copy-start.3
  26.0 58.4 %copy-start.6 = (f32[512,128]{1,0:T(8,128)S(1)}, f32[512,128]{1,0:T(8,128)}, u32[]{:S(2)}) copy-start(f32[512,128]{1,0:T(8,128)} %param.16) | copy-start | bytes 786436
  28.4 55.9 %reduce-scatter.5.cloned.1.call-start = ((), (), s32[]{:S(2)}) async-start(), calls=%async_computation.3 | async-start | bytes 786432 | tf_op jit(solution)/shard_map/reduce_scatter | solution.py:50
  74.9 56.5 %all-reduce.2.cloned.1.call-start = ((), (), s32[]{:S(2)}) async-start(), calls=%async_computation.4 | async-start | bytes 524288 | tf_op jit(solution)/shard_map/psum | solution.py:51
  84.4 156.6 %all-gather.2.cloned.1.call-start = ((), (), s32[]{:S(2)}) async-start(), calls=%async_computation.5 | async-start | bytes 5242880 | tf_op jit(solution)/shard_map/all_gather | solution.py:63
  153.5 0.8 copy-start.4
  157.2 7.5 %copy-start.5 = (f32[512,128]{0,1:T(8,128)S(1)}, f32[512,128]{0,1:T(8,128)}, u32[]{:S(2)}) copy-start(f32[512,128]{0,1:T(8,128)} %get-tuple-element.25) | copy-start | bytes 786436
Sparse Core Ops, SparseCore 0:
  28.5 46.3 reduce-scatter.2
  77.2 7.1 reduce-scatter.4
  87.3 44.1 all-reduce.1
  163.0 77.9 all-gather.1
where the time goes:
time: 255 us; the launch traced here: 254 us
  waiting for transfers between devices  167 us (65%)
  local copies, waits for them, and re-layouts  31 us (12%)
  blocking collectives  18.7 us (7%)
  between operations  14.6 us (6%)
  matrix products  12.8 us (5%)
  other arithmetic  9.72 us (4%)
    all_gather x1, waiting for transfers between devices, body(): lax.all_gather(weight_new.astype(jnp.bfloat16), 'fs', axis=1, tiled=True)  69.5 us
    reduce_scatter x1, waiting for transfers between devices, body(): lax.psum_scatter(split_product(out_cotangent, reduced, (((0,), (0,)), (()...  46.5 us
    psum x1, waiting for transfers between devices, body(): projected = lax.psum(proj_rows, 'rep')  41.6 us
    unnamed x27, local copies, waits for them, and re-layouts  24.9 us
    psum x1, blocking collectives, body(): energy = lax.psum(jnp.sum(direction * direction), ('fs', 'tp'))  16.5 us
    reduce_scatter x1, waiting for transfers between devices, body(): lax.psum_scatter(proj_rows, 'tp', scatter_dimension=1, tiled=True)  9.34 us
    dot_general x2, matrix products, split_product(): lax.dot_general(narrow, lower, numbers, preferred_element_type=jnp.float32)  8.03 us
    mul x1, local copies, waits for them, and re-layouts, head_output(): grouped * grouped  5.15 us
  transfers between devices with their start and end apart: 4, of which 4 were waited for; matrix products, arithmetic and copies ran while one was open for 6% of the time, Pallas kernels for 0%

commit v1 on v0

--- a/solution.py
+++ b/solution.py
@@ -60,7 +60,9 @@
         -1.0 / (spread + 1e-06)
     )
     weight_new = weight + step_out
-    weight_copy = lax.all_gather(weight_new.astype(jnp.bfloat16), "fs", axis=1, tiled=True)
+    x = weight_new.astype(jnp.bfloat16)
+    parts = lax.all_gather(x, "fs", axis=0, tiled=False)
+    weight_copy = jnp.concatenate(parts, axis=1)
     return (weight_new, weight_copy, step_out, first_new, second_new)
 
 

time: 255 us -> 272 us (1.067)
  local copies, waits for them, and re-layouts: 31 us -> 48.2 us
    reshape x0 -> x1, local copies, waits for them, and re-layouts: none -> 10.2 us  [body(): weight_copy = jnp.concatenate(parts, axis=1)]
    all_gather x0 -> x1, local copies, waits for them, and re-layouts: none -> 7.82 us  [body(): parts = lax.all_gather(x, 'fs', axis=0, tiled=False)]
  transfers between devices with their start and end apart: 4 -> 4, of which waited for: 4 -> 4; matrix products, arithmetic and copies ran while one was open for 6% -> 5% of each run, Pallas kernels for 0% -> 0%
where the time goes in v1:
time: 272 us; the launch traced here: 271 us
  waiting for transfers between devices  167 us (61%)
  local copies, waits for them, and re-layouts  48.2 us (18%)
  blocking collectives  18.7 us (7%)
  between operations  14.6 us (5%)
  matrix products  12.8 us (5%)
  other arithmetic  9.72 us (4%)
    all_gather x1, waiting for transfers between devices, body(): parts = lax.all_gather(x, 'fs', axis=0, tiled=False)  69.5 us
    reduce_scatter x1, waiting for transfers between devices, body(): lax.psum_scatter(split_product(out_cotangent, reduced, (((0,), (0,)), (()...  46.5 us
    psum x1, waiting for transfers between devices, body(): projected = lax.psum(proj_rows, 'rep')  41.6 us
    unnamed x27, local copies, waits for them, and re-layouts  24 us
    psum x1, blocking collectives, body(): energy = lax.psum(jnp.sum(direction * direction), ('fs', 'tp'))  16.5 us
    reshape x1, local copies, waits for them, and re-layouts, body(): weight_copy = jnp.concatenate(parts, axis=1)  10.2 us
    reduce_scatter x1, waiting for transfers between devices, body(): lax.psum_scatter(proj_rows, 'tp', scatter_dimension=1, tiled=True)  9.34 us
    dot_general x2, matrix products, split_product(): lax.dot_general(narrow, lower, numbers, preferred_element_type=jnp.float32)  8.03 us
  transfers between devices with their start and end apart: 4, of which 4 were waited for; matrix products, arithmetic and copies ran while one was open for 5% of the time, Pallas kernels for 0%

profile of v1, /device:TPU:0, one launch (start us, length us, event | category | flops | bytes accessed | tf_op | source)
XLA Modules:
  0.0 271.1 jit_solution(3114219503058571143)
XLA Ops:
  7.2 0.9 broadcast_bitcast_fusion.1
  8.1 0.7 broadcast_bitcast_fusion
  8.8 4.2 %fusion = f32[768,1024]{1,0:T(8,128)} fusion(bf16[768,1024]{1,0:T(8,128)(2,1)} %param.10, bf16[768,1024]{1,0:T(8,128)(2,1)} %param.9, f32[1024]{0:T(1024)S(1)} %bitcast.27), kind=kLoop, calls=%fused_computation.2 | loop fusion | flops 3932160 | bytes 6295552 | tf_op jit(solution)/shard_map/mul | solution.py:17
  13.0 5.2 %mul.92 = f32[768,4,256]{2,1,0:T(4,128)} reshape(f32[768,1024]{1,0:T(8,128)} %fusion) | data formatting | bytes 6291456 | tf_op jit(solution)/shard_map/mul | solution.py:17
  18.2 2.8 %reduce_sum.18 = f32[768,4]{1,0:T(8,128)S(1)} reduce(f32[768,4,256]{2,1,0:T(4,128)} %mul.92, f32[]{:T(128)} %constant.2.clone.1), dimensions={2}, to_apply=%region_0.0 | reduce | flops 783360 | bytes 3158020 | tf_op jit(solution)/shard_map/reduce_sum | solution.py:17
  21.1 1.0 mul.93
  22.1 0.8 copy.42
  22.8 0.6 copy-done.1
  23.5 0.5 copy-done.2
  24.0 0.9 fusion.2
  25.0 1.0 fusion.5
  26.0 2.4 fusion.1
  28.5 46.5 %reduce-scatter.3.cloned.1.call-done = f32[512,256]{0,1:T(8,128)} async-done(((f32[2048,256]{0,1:T(8,128)}), f32[512,256]{0,1:T(8,128)}) %reduce-scatter.3.cloned.1.call-update) | async-done | bytes 524304 | tf_op jit(solution)/shard_map/reduce_scatter | solution.py:44
  75.0 9.3 %reduce-scatter.5.cloned.1.call-done = f32[512,128]{0,1:T(8,128)} async-done(((f32[512,256]{0,1:T(8,128)}), f32[512,128]{0,1:T(8,128)}) %reduce-scatter.5.cloned.1.call-update) | async-done | bytes 262160 | tf_op jit(solution)/shard_map/reduce_scatter | solution.py:50
  84.4 0.8 copy.31
  85.2 1.8 copy.34
  87.0 2.9 %copy.35 = f32[1024,512]{0,1:T(8,128)} copy(f32[1024,512]{1,0:T(8,128)} %param.15) | data formatting | bytes 4194304 | tf_op args[6]
  89.9 41.6 %all-reduce.2.cloned.1.call-done = f32[512,128]{0,1:T(8,128)} async-done(((f32[512,128]{0,1:T(8,128)}), f32[512,128]{0,1:T(8,128)}) %all-reduce.2.cloned.1.call-update) | async-done | bytes 262160 | tf_op jit(solution)/shard_map/psum | solution.py:51
  131.5 2.6 multiply_reduce_fusion
  134.1 16.5 %psum.15 = f32[]{:T(128)} all-reduce(f32[]{:T(128)} %get-tuple-element.22), channel_id=1, replica_groups=mesh['fs'=4,'rep'=4,'tp'=2] {'fs','tp'}, use_global_device_ids=true, to_apply=%region_5.0 | all-reduce | flops 1 | bytes 8 | tf_op jit(solution)/shard_map/psum | solution.py:55
  151.3 2.2 all_gather.9
  153.5 0.8 copy-done.4
  154.3 2.8 %fusion.8 = f32[512,1024]{1,0:T(8,128)} fusion(bf16[1024,256]{1,0:T(8,128)(2,1)} %param.14, f32[512,256]{0,1:T(8,128)S(1)} %all_gather.9), kind=kOutput, calls=%fused_computation.19 | convolution fusion | flops 268566528 | bytes 3145728 | tf_op jit(solution)/shard_map/dot_general | solution.py:25
  157.2 5.7 %fusion.11 = (bf16[1024,512]{0,1:T(8,128)(2,1)}, f32[1024,512]{0,1:T(8,128)}, f32[1024,512]{0,1:T(8,128)}) fusion(f32[1024,512]{0,1:T(8,128)} %copy.35, f32[]{:T(128)S(6)} %div.19, f32[512,1024]{1,0:T(8,128)} %fusion.8, bf16[1024,256]{1,0:T(8,128)(2,1)} %param.14, f32[512,256]{0,1:T(8,128)} %copy-done.4), kind=kOutput, calls=%fused_computation.24 | convolution fusion | flops 271056896 | bytes 10485764 | tf_op jit(solution)/shard_map/dot_general | solution.py:27
  162.9 1.8 copy.40
  164.7 0.8 copy.39
  165.5 3.0 %copy.37 = f32[1024,512]{1,0:T(8,128)} copy(f32[1024,512]{0,1:T(8,128)} %get-tuple-element.21) | data formatting | bytes 4194304
  168.5 3.0 %copy.38 = f32[1024,512]{1,0:T(8,128)} copy(f32[1024,512]{0,1:T(8,128)} %get-tuple-element.26) | data formatting | bytes 4194304
  171.5 69.5 %all-gather.3.cloned.1.call-done = bf16[4096,512]{0,1:T(8,128)(2,1)} async-done(((bf16[1024,512]{0,1:T(8,128)(2,1)}), bf16[4096,512]{0,1:T(8,128)(2,1)}) %all-gather.3.cloned.1.call-update) | async-done | bytes 4194320 | tf_op jit(solution)/shard_map/all_gather | solution.py:64
  241.0 7.8 %reshape.33 = bf16[4,1024,512]{1,0,2:T(4,128)(2,1)} reshape(bf16[4096,512]{0,1:T(8,128)(2,1)} %all-gather.3.cloned.1.call-done) | data formatting | bytes 8388608 | tf_op jit(solution)/shard_map/all_gather | solution.py:64
  248.8 10.2 %copy.36 = bf16[1024,4,512]{2,1,0:T(4,128)(2,1)} copy(bf16[1024,4,512]{0,1,2:T(4,128)(2,1)} %bitcast.22) | data formatting | bytes 8388608 | tf_op jit(solution)/shard_map/reshape | solution.py:65
  259.0 5.6 %copy.44 = bf16[128,8,4,512]{3,1,2,0:T(8,128)(2,1)} copy(bf16[128,8,4,512]{3,2,1,0:T(4,128)(2,1)} %bitcast.23) | data formatting | bytes 8388608
  (22 shorter events, 0.4 us)
Async XLA Ops:
  7.2 17.8 %copy-start = (bf16[768,2048]{1,0:T(8,128)(2,1)S(1)}, bf16[768,2048]{1,0:T(8,128)(2,1)}, u32[]{:S(2)}) copy-start(bf16[768,2048]{1,0:T(8,128)(2,1)} %param.13) | copy-start | bytes 9437188
  7.2 67.7 %reduce-scatter.3.cloned.1.call-start = ((), (), s32[]{:S(2)}) async-start(), calls=%async_computation.2 | async-start | bytes 2621440 | tf_op jit(solution)/shard_map/reduce_scatter | solution.py:44
  22.0 1.4 copy-start.1
  22.1 1.9 copy-start.2
  22.1 2.0 copy-start.3
  26.0 58.4 %copy-start.6 = (f32[512,128]{1,0:T(8,128)S(1)}, f32[512,128]{1,0:T(8,128)}, u32[]{:S(2)}) copy-start(f32[512,128]{1,0:T(8,128)} %param.16) | copy-start | bytes 786436
  28.4 55.9 %reduce-scatter.5.cloned.1.call-start = ((), (), s32[]{:S(2)}) async-start(), calls=%async_computation.3 | async-start | bytes 786432 | tf_op jit(solution)/shard_map/reduce_scatter | solution.py:50
  74.9 56.5 %all-reduce.2.cloned.1.call-start = ((), (), s32[]{:S(2)}) async-start(), calls=%async_computation.4 | async-start | bytes 524288 | tf_op jit(solution)/shard_map/psum | solution.py:51
  84.4 156.6 %all-gather.3.cloned.1.call-start = ((), (), s32[]{:S(2)}) async-start(), calls=%async_computation.5 | async-start | bytes 5242880 | tf_op jit(solution)/shard_map/all_gather | solution.py:64
  153.5 0.8 copy-start.4
  157.2 7.5 %copy-start.5 = (f32[512,128]{0,1:T(8,128)S(1)}, f32[512,128]{0,1:T(8,128)}, u32[]{:S(2)}) copy-start(f32[512,128]{0,1:T(8,128)} %get-tuple-element.25) | copy-start | bytes 786436
Sparse Core Ops, SparseCore 0:
  28.5 46.3 reduce-scatter.2
  77.2 7.1 reduce-scatter.4
  87.3 44.1 all-reduce.1
  163.0 77.9 all-gather.2
